TPU v7x, 32 devices: a whole 2x2x4 slice. The times are simulated.
32 devices in a mesh: grp: 2 (over y), sp: 4 (over z), tp: 4 (over x, core).
Axes of the slice: x: 2, y: 2, z: 4, core: 2. Of those that a mesh axis runs over, the one named last changes fastest.
Arguments:
- query_rows: bfloat16 [1024, 1024], P(('grp', 'sp'), 'tp'), parts along dimension 0, may hold values from -12 to 12
- key_rows: bfloat16 [1024, 1024], P(('grp', 'sp'), 'tp'), parts along dimension 0, may hold values from -9 to 9
- value_rows: bfloat16 [1024, 1024], P(('grp', 'sp'), 'tp'), parts along dimension 0, may hold values from -6 to 6
- key_logit: bfloat16 [1024, 8], P(('grp', 'sp'), 'tp'), parts along dimension 0, as said below
- residual: bfloat16 [1024, 2048], P(('grp', 'sp')), parts along dimension 0, may hold values from -6 to 6
- out_weight: bfloat16 [1024, 2048], P('tp'), may hold values from -0.1875 to 0.1875
- mix_gain: float32 [2048], replicated, may hold values from 0.1 to 1.9
- ffn_gain: float32 [2048], replicated, may hold values from 0.1 to 1.9
- out_gain: float32 [2048], replicated, may hold values from 0.1 to 1.9
- gate_weight: bfloat16 [2048, 5120], P('sp', 'tp'), may hold values from -0.125 to 0.125
- up_weight: bfloat16 [2048, 5120], P('sp', 'tp'), may hold values from -0.125 to 0.125
- down_weight: bfloat16 [2048, 5120], P('sp', 'tp'), may hold values from -0.078125 to 0.078125
Outputs:
- layer_out: bfloat16 [1024, 2048], P(('grp', 'sp')), parts along dimension 0
There are 2 independent parts, one for each index of `grp`. A program takes and returns all parts, laid end to end along the dimension named above; an argument that names none is the same for every part. Nothing has to cross between parts.
Inputs may be any that keep to these rules, and one draw needn't show every extreme that they name: `key_logit`: log-odds offsets of the keys, all negative.
All inputs are finite; a program needn't handle non-finite values.
Results may differ from a plain program's by a relative error of at most 0.018.
Values may be sent and summed in bfloat16 or wider, within the bound.
No kernel may reach another device: no remote copies, remote signals or barrier semaphores. Data moves between devices by JAX's collectives and lax.ppermute only.
A program may use at most 64 MiB of HBM per device.

v0:
```python
import jax
import jax.numpy as jnp
from jax import lax
from jax.sharding import PartitionSpec as P

epsilon = 1e-06


def normalize(payload_table):
    return payload_table * lax.rsqrt(
        jnp.mean(payload_table * payload_table, axis=-1, keepdims=True) + epsilon
    )


def shards(
    query_rows,
    key_rows,
    value_rows,
    key_logit,
    residual,
    out_weight,
    mix_gain,
    ffn_gain,
    out_gain,
    gate_weight,
    up_weight,
    down_weight,
):
    tok_rows = query_rows.shape[0]
    head_count = key_logit.shape[1]
    head_width = query_rows.shape[1] // head_count
    block_count = lax.axis_size("sp")
    own_block = lax.axis_index("sp")
    queries = query_rows.reshape(tok_rows, head_count, head_width).transpose(1, 0, 2)
    score_scale = head_width ** (-0.5)
    query_pos = own_block * tok_rows + jnp.arange(tok_rows, dtype=jnp.int32)[:, None]

    def group_terms(key_part, value_part, logit_part, first_block):
        span_rows = key_part.shape[0]
        shard_count = span_rows // tok_rows

        def compute(unused):
            scores = (
                jnp.einsum(
                    "hqd,khd->hqk",
                    queries,
                    key_part.reshape(span_rows, head_count, head_width),
                    preferred_element_type=jnp.float32,
                )
                * score_scale
            )
            scores = scores + jnp.transpose(logit_part.astype(jnp.float32))[:, None, :]
            key_pos = first_block * tok_rows + jnp.arange(span_rows, dtype=jnp.int32)[None, :]
            causal = (key_pos < query_pos).reshape(tok_rows, shard_count, tok_rows)
            scores = scores.reshape(head_count, tok_rows, shard_count, tok_rows)
            keep_log = jnp.where(causal, jax.nn.log_sigmoid(-scores), 0.0)
            within = lax.cumsum(keep_log, axis=3, reverse=True) - keep_log
            sticks = jnp.where(causal, jnp.exp(jax.nn.log_sigmoid(scores) + within), 0.0).astype(
                jnp.bfloat16
            )
            partials = jnp.einsum(
                "hqgk,gkhd->ghqd",
                sticks,
                value_part.reshape(shard_count, tok_rows, head_count, head_width),
                preferred_element_type=jnp.float32,
            )
            return (jnp.sum(keep_log, axis=3), partials)

        def skipped(unused):
            return (
                jnp.zeros((head_count, tok_rows, shard_count), jnp.float32),
                jnp.zeros((shard_count, head_count, tok_rows, head_width), jnp.float32),
            )

        return lax.cond(first_block <= own_block, compute, skipped, 0)

    initial = (
        jnp.zeros((head_count, tok_rows, block_count), jnp.float32),
        jnp.zeros((block_count, head_count, tok_rows, head_width), jnp.float32),
    )
    tables = initial
    key_part = lax.all_gather(key_rows, "sp", axis=0, tiled=True)
    value_part = lax.all_gather(value_rows, "sp", axis=0, tiled=True)
    logit_part = lax.all_gather(key_logit, "sp", axis=0, tiled=True)
    shard_count = key_part.shape[0] // tok_rows
    group_size = 2
    span_rows = group_size * tok_rows

    def one_group(carried, group_index):
        offset = group_index * span_rows
        first_block = group_index * group_size
        totals, partials = group_terms(
            lax.dynamic_slice_in_dim(key_part, offset, span_rows, 0),
            lax.dynamic_slice_in_dim(value_part, offset, span_rows, 0),
            lax.dynamic_slice_in_dim(logit_part, offset, span_rows, 0),
            first_block,
        )
        carried = (
            lax.dynamic_update_slice(carried[0], totals, (0, 0, first_block)),
            lax.dynamic_update_slice(carried[1], partials, (first_block, 0, 0, 0)),
        )
        return (carried, None)

    tables, unused = lax.scan(
        one_group, tables, jnp.arange(shard_count // group_size, dtype=jnp.int32)
    )
    totals, partials = tables
    suffix = lax.cumsum(totals, axis=2, reverse=True) - totals
    attended = jnp.einsum(
        "hqb,bhqd->qhd", jnp.exp(suffix), partials, precision=lax.Precision.HIGHEST
    )
    attended = attended.reshape(tok_rows, head_count * head_width).astype(jnp.bfloat16)
    head_part = jnp.dot(attended, out_weight, preferred_element_type=jnp.float32)
    mixed_rows = lax.psum(head_part.astype(jnp.bfloat16), "tp")
    middle = (
        residual.astype(jnp.float32) + mix_gain * normalize(mixed_rows.astype(jnp.float32))
    ).astype(jnp.bfloat16)
    normed = (ffn_gain * normalize(middle.astype(jnp.float32))).astype(jnp.bfloat16)
    gate_act = jnp.dot(
        normed,
        lax.all_gather(gate_weight, "sp", axis=0, tiled=True),
        preferred_element_type=jnp.float32,
    )
    up_act = jnp.dot(
        normed,
        lax.all_gather(up_weight, "sp", axis=0, tiled=True),
        preferred_element_type=jnp.float32,
    )
    hidden = (jax.nn.silu(gate_act) * up_act).astype(jnp.bfloat16)
    unit_part = lax.dot_general(
        hidden,
        lax.all_gather(down_weight, "sp", axis=0, tiled=True),
        (((1,), (1,)), ((), ())),
        preferred_element_type=jnp.float32,
    )
    ffn_out = lax.psum(unit_part.astype(jnp.bfloat16), "tp")
    return (middle.astype(jnp.float32) + out_gain * normalize(ffn_out.astype(jnp.float32))).astype(
        jnp.bfloat16
    )


def solution(mesh):
    placed = (
        P(("grp", "sp"), "tp"),
        P(("grp", "sp"), "tp"),
        P(("grp", "sp"), "tp"),
        P(("grp", "sp"), "tp"),
        P(("grp", "sp"), None),
        P("tp", None),
        P(),
        P(),
        P(),
        P("sp", "tp"),
        P("sp", "tp"),
        P("sp", "tp"),
    )
    return jax.shard_map(
        shards, mesh=mesh, in_specs=placed, out_specs=P(("grp", "sp"), None), check_vma=False
    )
```

profile of v0, /device:TPU:0, one launch (start us, length us, event | category | flops | bytes accessed | tf_op | source)
XLA Modules:
  0.0 408.5 jit_solution(9131922966451456633)
XLA Ops:
  7.4 1.0 copy.41
  8.4 14.5 %all_gather.18 = bf16[512,256]{0,1:T(8,128)(2,1)S(1)} all-gather(bf16[128,256]{0,1:T(8,128)(2,1)S(1)} %copy.41), channel_id=1, replica_groups=mesh['grp'=2,'sp'=4,'tp'=4] {'sp'}, dimensions={0}, use_global_device_ids=true | all-gather | bytes 327680 | tf_op jit(solution)/shard_map/all_gather | solution.py:82
  22.9 14.6 %all_gather.20 = bf16[512,256]{1,0:T(8,128)(2,1)S(1)} all-gather(bf16[128,256]{1,0:T(8,128)(2,1)} %param.18), channel_id=1, replica_groups=mesh['grp'=2,'sp'=4,'tp'=4] {'sp'}, dimensions={0}, use_global_device_ids=true | all-gather | bytes 327680 | tf_op jit(solution)/shard_map/all_gather | solution.py:83
  37.5 0.9 copy.42
  38.4 0.1 copy.43
  38.6 10.0 %all_gather.19 = bf16[512,2]{0,1:T(2,128)(2,1)S(1)} all-gather(bf16[128,2]{0,1:T(2,128)(2,1)} %param.19), channel_id=1, replica_groups=mesh['grp'=2,'sp'=4,'tp'=4] {'sp'}, dimensions={0}, use_global_device_ids=true | all-gather | bytes 2560 | tf_op jit(solution)/shard_map/all_gather | solution.py:84
  48.6 0.1 broadcast_in_dim.28.clone
  48.7 8.5 %while.13 = (s32[]{:T(128)}, f32[2,128,4]{1,2,0:T(4,128)S(1)}, f32[4,2,128,128]{3,0,1,2:T(4,128)S(1)}, s32[2]{0:T(128)S(1)}, s32[]{:T(128)}, /*index=5*/bf16[512...) while((s32[]{:T(128)}, f32[2,128,4]{1,2,0:T(4,128)S(1)}, ...), condition=%wide.region_5.6_spmd.clone, body=%wide.region_0.5_spmd.clone.sunk | while | flops 43418504 | bytes 4373875 | solution.py:104
  48.7 0.6 dynamic_slice.39
  49.9 5.3 %conditional.3 = (f32[2,128,2]{1,2,0:T(2,128)S(1)}, f32[2,2,128,128]{3,2,1,0:T(8,128)S(1)}) conditional(s32[]{:T(128)} %convert_element_type.116, () %tuple.48, (s32[]{:T(128)}, s32[]{:T(128)}, s32[]{:T(128)}, bf16[512,256]{0,1:T(8,128)(2,1)S(1)}, bf16[2,128,128]{2,1,0:T(8,128)(2,1)S(1)}, /*index=5*/bf16[512,2]{0,1:T(2,128)(2,1)S(1)}, ...), branch_computations={%region_1.1_spmd, %region_2.4_spmd} | conditional | flops 43418500 | bytes 3844702 | solution.py:75
  50.6 0.2 fusion.2
  50.9 0.2 broadcast_compare_fusion
  51.1 0.8 fusion.35
  51.9 2.2 fusion.38
  54.0 0.9 select_convert_fusion
  55.0 0.2 fusion.8
  55.2 0.3 copy_dynamic-update-slice_fusion.2
  55.6 0.6 dynamic_slice.39
  56.9 0.3 copy_dynamic-update-slice_fusion.2
  57.2 0.0 copy-start.1
  57.2 0.0 copy-start.2
  57.2 0.0 copy-start.3
  57.3 0.2 copy.45
  57.5 1.8 fusion.39
  59.3 1.1 convolution_convert_fusion.1
  60.4 0.0 all-reduce.3.cloned.1.call-update
  60.4 0.0 all-gather.4.cloned.1.call-start
  60.5 0.5 all-gather.4.cloned.1.call-update
  61.0 0.0 all-gather.6.cloned.1.call-start
  61.1 0.5 all-gather.6.cloned.1.call-update
  61.6 0.0 all-gather.8.cloned.1.call-start
  61.7 0.5 all-gather.8.cloned.1.call-update
  62.2 0.0 all-reduce.5.cloned.1.call-start
  62.2 34.5 %all-reduce.3.cloned.1.call-done = bf16[128,2048]{1,0:T(8,128)(2,1)} async-done(((bf16[128,2048]{1,0:T(8,128)(2,1)}), bf16[128,2048]{1,0:T(8,128)(2,1)}) %all-reduce.3.cloned.1.call-update) | async-done | bytes 524304 | tf_op jit(solution)/shard_map/psum | solution.py:114
  96.8 1.2 fusion.12
  98.0 0.0 copy-done.1
  98.0 0.0 copy-done.2
  98.0 1.5 fusion.18
  99.5 63.6 %all-gather.4.cloned.1.call-done = bf16[2048,1280]{1,0:T(8,128)(2,1)} async-done(((bf16[512,1280]{1,0:T(8,128)(2,1)}), bf16[2048,1280]{1,0:T(8,128)(2,1)}) %all-gather.4.cloned.1.call-update) | async-done | bytes 5242896 | tf_op jit(solution)/shard_map/all_gather | solution.py:121
  163.1 3.4 fusion.30
  166.5 0.0 copy-start.4
  166.5 94.3 %all-gather.6.cloned.1.call-done = bf16[2048,1280]{1,0:T(8,128)(2,1)} async-done(((bf16[512,1280]{1,0:T(8,128)(2,1)}), bf16[2048,1280]{1,0:T(8,128)(2,1)}) %all-gather.6.cloned.1.call-update) | async-done | bytes 5242896 | tf_op jit(solution)/shard_map/all_gather | solution.py:126
  260.8 97.7 %all-gather.8.cloned.1.call-done = bf16[2048,1280]{1,0:T(8,128)(2,1)} async-done(((bf16[512,1280]{1,0:T(8,128)(2,1)}), bf16[2048,1280]{1,0:T(8,128)(2,1)}) %all-gather.8.cloned.1.call-update) | async-done | bytes 5242896 | tf_op jit(solution)/shard_map/all_gather | solution.py:132
  358.5 7.2 %convolution_convert_fusion = bf16[128,2048]{1,0:T(8,128)(2,1)} fusion(bf16[2048,1280]{1,0:T(8,128)(2,1)} %all-gather.8.cloned.1.call-done, bf16[2048,1280]{1,0:T(8,128)(2,1)} %all-gather.6.cloned.1.call-done, f32[128,1280]{1,0:T(8,128)S(1)} %fusion.30, bf16[128,2048]{1,0:T(8,128)(2,1)S(1)} %get-tuple-element.241, f32[128]{0:T(128)S(1)} %add_rsqrt_fusion.1, ...), kind=kOutput, calls=%fused_computation.23 | convolution fusion | flops 1344471040 | bytes 12198400 | tf_op jit(solution)/shard_map/dot_general | solution.py:130
  365.7 0.0 all-reduce.5.cloned.1.call-update
  365.7 31.9 %all-reduce.5.cloned.1.call-done = bf16[128,2048]{1,0:T(8,128)(2,1)} async-done(((bf16[128,2048]{1,0:T(8,128)(2,1)}), bf16[128,2048]{1,0:T(8,128)(2,1)}) %all-reduce.5.cloned.1.call-update) | async-done | bytes 524304 | tf_op jit(solution)/shard_map/psum | solution.py:136
  397.6 1.2 fusion.16
  398.9 2.1 fusion.21
  (26 shorter events, 0.3 us)
Async XLA Ops:
  7.4 51.9 %copy-start = (bf16[256,2048]{1,0:T(8,128)(2,1)S(1)}, bf16[256,2048]{1,0:T(8,128)(2,1)}, u32[]{:S(2)}) copy-start(bf16[256,2048]{1,0:T(8,128)(2,1)} %param.21) | copy-start | bytes 3145732
  7.4 89.4 %all-reduce.3.cloned.1.call-start = ((), (), s32[]{:S(2)}) async-start(), calls=%async_computation | async-start | bytes 1048576 | tf_op jit(solution)/shard_map/psum | solution.py:114
  57.2 40.8 %copy-start.1 = (bf16[128,2048]{1,0:T(8,128)(2,1)S(1)}, bf16[128,2048]{1,0:T(8,128)(2,1)}, u32[]{:S(2)}) copy-start(bf16[128,2048]{1,0:T(8,128)(2,1)} %param.20) | copy-start | bytes 1572868
  57.2 40.8 %copy-start.2 = (f32[2048]{0:T(1024)S(1)}, f32[2048]{0:T(1024)}, u32[]{:S(2)}) copy-start(f32[2048]{0:T(1024)} %param.22) | copy-start | bytes 24580
  57.2 105.8 %copy-start.3 = (f32[2048]{0:T(1024)S(1)}, f32[2048]{0:T(1024)}, u32[]{:S(2)}) copy-start(f32[2048]{0:T(1024)} %param.23) | copy-start | bytes 24580
  60.4 102.6 %all-gather.4.cloned.1.call-start = ((), (), s32[]{:S(2)}) async-start(), calls=%async_computation.1 | async-start | bytes 6553600 | tf_op jit(solution)/shard_map/all_gather | solution.py:121
  61.0 199.8 %all-gather.6.cloned.1.call-start = ((), (), s32[]{:S(2)}) async-start(), calls=%async_computation.2 | async-start | bytes 6553600 | tf_op jit(solution)/shard_map/all_gather | solution.py:126
  61.6 296.9 %all-gather.8.cloned.1.call-start = ((), (), s32[]{:S(2)}) async-start(), calls=%async_computation.3 | async-start | bytes 6553600 | tf_op jit(solution)/shard_map/all_gather | solution.py:132
  62.2 335.4 %all-reduce.5.cloned.1.call-start = ((), (), s32[]{:S(2)}) async-start(), calls=%async_computation.4 | async-start | bytes 1048576 | tf_op jit(solution)/shard_map/psum | solution.py:136
  166.5 232.4 %copy-start.4 = (f32[2048]{0:T(1024)S(1)}, f32[2048]{0:T(1024)}, u32[]{:S(2)}) copy-start(f32[2048]{0:T(1024)} %param.24) | copy-start | bytes 24580
Sparse Core Ops, SparseCore 0:
  60.6 36.1 all-reduce.2
  365.9 31.7 all-reduce.4
Sparse Core Ops, SparseCore 1:
  62.5 100.5 all-gather.3
  164.5 96.2 all-gather.5
  262.2 96.2 all-gather.7
where the time goes:
time: 409 us
  waiting for transfers between devices  324 us (79%)
  blocking collectives  39.1 us (10%)
  between operations  15.1 us (4%)
  matrix products  14 us (3%)
  other arithmetic  10.2 us (2%)
  local copies, waits for them, and re-layouts  4.28 us (1%)
    all_gather x1, waiting for transfers between devices, shards(): lax.all_gather(down_weight, 'sp', axis=0, tiled=True)  97.7 us
    all_gather x1, waiting for transfers between devices, shards(): lax.all_gather(up_weight, 'sp', axis=0, tiled=True)  94.3 us
    all_gather x1, waiting for transfers between devices, shards(): lax.all_gather(gate_weight, 'sp', axis=0, tiled=True)  63.6 us
    psum x1, waiting for transfers between devices, shards(): mixed_rows = lax.psum(head_part.astype(jnp.bfloat16), 'tp')  34.5 us
    psum x1, waiting for transfers between devices, shards(): ffn_out = lax.psum(unit_part.astype(jnp.bfloat16), 'tp')  31.9 us
    all_gather x1, blocking collectives, shards(): value_part = lax.all_gather(value_rows, 'sp', axis=0, tiled=True)  14.6 us
    all_gather x1, blocking collectives, shards(): key_part = lax.all_gather(key_rows, 'sp', axis=0, tiled=True)  14.5 us
    all_gather x1, blocking collectives, shards(): logit_part = lax.all_gather(key_logit, 'sp', axis=0, tiled=True)  10 us
  transfers between devices with their start and end apart: 5, of which 5 were waited for; matrix products, arithmetic and copies ran while one was open for 1% of the time, Pallas kernels for 0%

commit v1 on v0

--- a/solution.py
+++ b/solution.py
@@ -111,7 +111,7 @@
     )
     attended = attended.reshape(tok_rows, head_count * head_width).astype(jnp.bfloat16)
     head_part = jnp.dot(attended, out_weight, preferred_element_type=jnp.float32)
-    mixed_rows = lax.psum(head_part.astype(jnp.bfloat16), "tp")
+    mixed_rows = jnp.sum(lax.all_gather(head_part.astype(jnp.bfloat16), "tp"), axis=0)
     middle = (
         residual.astype(jnp.float32) + mix_gain * normalize(mixed_rows.astype(jnp.float32))
     ).astype(jnp.bfloat16)

time: 409 us -> 430 us (1.051)
  waiting for transfers between devices: 324 us -> 346 us
    psum x1 -> x0, waiting for transfers between devices: 34.5 us -> none  [shards(): mixed_rows = lax.psum(head_part.astype(jnp.bfloat16), 'tp')]
    all_gather x1, waiting for transfers between devices: 63.6 us -> 97 us  [shards(): lax.all_gather(gate_weight, 'sp', axis=0, tiled=True)]
    all_gather x0 -> x1, waiting for transfers between devices: none -> 23.1 us  [shards(): lax.all_gather(head_part.astype(jnp.bfloat16), 'tp')]
where the time goes in v1:
time: 430 us; the launch traced here: 429 us
  waiting for transfers between devices  346 us (80%)
  blocking collectives  39.1 us (9%)
  matrix products  14 us (3%)
  between operations  13.3 us (3%)
  other arithmetic  10.1 us (2%)
    all_gather x1, waiting for transfers between devices, shards(): lax.all_gather(up_weight, 'sp', axis=0, tiled=True)  97.8 us
    all_gather x1, waiting for transfers between devices, shards(): lax.all_gather(gate_weight, 'sp', axis=0, tiled=True)  97 us
    all_gather x1, waiting for transfers between devices, shards(): lax.all_gather(down_weight, 'sp', axis=0, tiled=True)  94.6 us
    psum x1, waiting for transfers between devices, shards(): ffn_out = lax.psum(unit_part.astype(jnp.bfloat16), 'tp')  31.9 us
    all_gather x1, waiting for transfers between devices, shards(): lax.all_gather(head_part.astype(jnp.bfloat16), 'tp')  23.1 us
    all_gather x1, blocking collectives, shards(): value_part = lax.all_gather(value_rows, 'sp', axis=0, tiled=True)  14.6 us
    all_gather x1, blocking collectives, shards(): key_part = lax.all_gather(key_rows, 'sp', axis=0, tiled=True)  14.5 us
    all_gather x1, blocking collectives, shards(): logit_part = lax.all_gather(key_logit, 'sp', axis=0, tiled=True)  10 us
  transfers between devices with their start and end apart: 5, of which 5 were waited for; matrix products, arithmetic and copies ran while one was open for 1% of the time, Pallas kernels for 0%

profile of v1, /device:TPU:0, one launch (start us, length us, event | category | flops | bytes accessed | tf_op | source)
XLA Modules:
  0.0 429.4 jit_solution(2671783025213710686)
XLA Ops:
  6.5 0.0 all-gather.12.cloned.1.call-start
  6.5 1.0 copy.41
  7.6 14.5 %all_gather.24 = bf16[512,256]{0,1:T(8,128)(2,1)S(1)} all-gather(bf16[128,256]{0,1:T(8,128)(2,1)S(1)} %copy.41), channel_id=1, replica_groups=mesh['grp'=2,'sp'=4,'tp'=4] {'sp'}, dimensions={0}, use_global_device_ids=true | all-gather | bytes 327680 | tf_op jit(solution)/shard_map/all_gather | solution.py:82
  22.1 14.6 %all_gather.26 = bf16[512,256]{1,0:T(8,128)(2,1)S(1)} all-gather(bf16[128,256]{1,0:T(8,128)(2,1)} %param.18), channel_id=1, replica_groups=mesh['grp'=2,'sp'=4,'tp'=4] {'sp'}, dimensions={0}, use_global_device_ids=true | all-gather | bytes 327680 | tf_op jit(solution)/shard_map/all_gather | solution.py:83
  36.6 0.9 copy.42
  37.6 0.1 copy.43
  37.7 10.0 %all_gather.25 = bf16[512,2]{0,1:T(2,128)(2,1)S(1)} all-gather(bf16[128,2]{0,1:T(2,128)(2,1)} %param.19), channel_id=1, replica_groups=mesh['grp'=2,'sp'=4,'tp'=4] {'sp'}, dimensions={0}, use_global_device_ids=true | all-gather | bytes 2560 | tf_op jit(solution)/shard_map/all_gather | solution.py:84
  47.8 0.1 broadcast_in_dim.28.clone
  47.8 8.5 %while.13 = (s32[]{:T(128)}, f32[2,128,4]{1,2,0:T(4,128)S(1)}, f32[4,2,128,128]{3,0,1,2:T(4,128)S(1)}, s32[2]{0:T(128)S(1)}, s32[]{:T(128)}, /*index=5*/bf16[512...) while((s32[]{:T(128)}, f32[2,128,4]{1,2,0:T(4,128)S(1)}, ...), condition=%wide.region_5.6_spmd.clone, body=%wide.region_0.5_spmd.clone.sunk | while | flops 43418504 | bytes 4373875 | solution.py:104
  47.9 0.6 dynamic_slice.39
  49.1 5.3 %conditional.3 = (f32[2,128,2]{1,2,0:T(2,128)S(1)}, f32[2,2,128,128]{3,2,1,0:T(8,128)S(1)}) conditional(s32[]{:T(128)} %convert_element_type.118, () %tuple.48, (s32[]{:T(128)}, s32[]{:T(128)}, s32[]{:T(128)}, bf16[512,256]{0,1:T(8,128)(2,1)S(1)}, bf16[2,128,128]{2,1,0:T(8,128)(2,1)S(1)}, /*index=5*/bf16[512,2]{0,1:T(2,128)(2,1)S(1)}, ...), branch_computations={%region_1.1_spmd, %region_2.4_spmd} | conditional | flops 43418500 | bytes 3844702 | solution.py:75
  49.8 0.2 fusion.2
  50.1 0.2 broadcast_compare_fusion
  50.3 0.8 fusion.35
  51.0 2.2 fusion.38
  53.2 0.9 select_convert_fusion
  54.2 0.2 fusion.8
  54.4 0.3 copy_dynamic-update-slice_fusion.2
  54.7 0.6 dynamic_slice.39
  56.0 0.3 copy_dynamic-update-slice_fusion.2
  56.4 0.2 copy.45
  56.6 0.0 copy-start.1
  56.6 0.0 copy-start.2
  56.6 1.8 fusion.39
  58.5 0.0 copy-start.3
  58.5 1.1 convolution_convert_fusion.1
  59.6 0.0 all-gather.12.cloned.1.call-update
  59.6 0.0 all-gather.6.cloned.1.call-start
  59.7 0.7 all-gather.6.cloned.1.call-update
  60.4 0.0 all-gather.10.cloned.1.call-start
  60.4 0.7 all-gather.10.cloned.1.call-update
  61.1 0.0 all-gather.8.cloned.1.call-start
  61.1 0.5 all-gather.8.cloned.1.call-update
  61.7 0.2 all-reduce.2.cloned.1.call-start
  61.9 23.1 %all-gather.12.cloned.1.call-done = bf16[512,2048]{1,0:T(8,128)(2,1)} async-done(((bf16[128,2048]{1,0:T(8,128)(2,1)}), bf16[512,2048]{1,0:T(8,128)(2,1)}) %all-gather.12.cloned.1.call-update) | async-done | bytes 2097168 | tf_op jit(solution)/shard_map/all_gather | solution.py:114
  85.0 2.0 reduce_sum.52
  87.0 0.2 fusion.12
  87.2 0.4 fusion.18
  87.6 97.0 %all-gather.6.cloned.1.call-done = bf16[2048,1280]{1,0:T(8,128)(2,1)} async-done(((bf16[512,1280]{1,0:T(8,128)(2,1)}), bf16[2048,1280]{1,0:T(8,128)(2,1)}) %all-gather.6.cloned.1.call-update) | async-done | bytes 5242896 | tf_op jit(solution)/shard_map/all_gather | solution.py:121
  184.6 3.4 fusion.30
  188.0 0.0 copy-start.4
  188.0 94.6 %all-gather.10.cloned.1.call-done = bf16[2048,1280]{1,0:T(8,128)(2,1)} async-done(((bf16[512,1280]{1,0:T(8,128)(2,1)}), bf16[2048,1280]{1,0:T(8,128)(2,1)}) %all-gather.10.cloned.1.call-update) | async-done | bytes 5242896 | tf_op jit(solution)/shard_map/all_gather | solution.py:132
  282.6 97.8 %all-gather.8.cloned.1.call-done = bf16[2048,1280]{1,0:T(8,128)(2,1)} async-done(((bf16[512,1280]{1,0:T(8,128)(2,1)}), bf16[2048,1280]{1,0:T(8,128)(2,1)}) %all-gather.8.cloned.1.call-update) | async-done | bytes 5242896 | tf_op jit(solution)/shard_map/all_gather | solution.py:126
  380.4 7.2 %convolution_convert_fusion = bf16[128,2048]{1,0:T(8,128)(2,1)} fusion(bf16[2048,1280]{1,0:T(8,128)(2,1)} %all-gather.10.cloned.1.call-done, bf16[2048,1280]{1,0:T(8,128)(2,1)} %all-gather.8.cloned.1.call-done, f32[128,1280]{1,0:T(8,128)S(1)} %fusion.30, bf16[128,2048]{1,0:T(8,128)(2,1)S(1)} %get-tuple-element.241, f32[128]{0:T(128)S(1)} %add_rsqrt_fusion.1, ...), kind=kOutput, calls=%fused_computation.23 | convolution fusion | flops 1344471040 | bytes 12198400 | tf_op jit(solution)/shard_map/dot_general | solution.py:130
  387.7 0.0 all-reduce.2.cloned.1.call-update
  387.7 31.9 %all-reduce.2.cloned.1.call-done = bf16[128,2048]{1,0:T(8,128)(2,1)} async-done(((bf16[128,2048]{1,0:T(8,128)(2,1)}), bf16[128,2048]{1,0:T(8,128)(2,1)}) %all-reduce.2.cloned.1.call-update) | async-done | bytes 524304 | tf_op jit(solution)/shard_map/psum | solution.py:136
  419.6 1.2 fusion.16
  420.8 2.1 fusion.21
  (27 shorter events, 0.3 us)
Async XLA Ops:
  6.5 51.9 %copy-start = (bf16[256,2048]{1,0:T(8,128)(2,1)S(1)}, bf16[256,2048]{1,0:T(8,128)(2,1)}, u32[]{:S(2)}) copy-start(bf16[256,2048]{1,0:T(8,128)(2,1)} %param.21) | copy-start | bytes 3145732
  6.5 78.4 %all-gather.12.cloned.1.call-start = ((), (), s32[]{:S(2)}) async-start(), calls=%async_computation.4 | async-start | bytes 2621440 | tf_op jit(solution)/shard_map/all_gather | solution.py:114
  56.6 30.6 %copy-start.1 = (bf16[128,2048]{1,0:T(8,128)(2,1)S(1)}, bf16[128,2048]{1,0:T(8,128)(2,1)}, u32[]{:S(2)}) copy-start(bf16[128,2048]{1,0:T(8,128)(2,1)} %param.20) | copy-start | bytes 1572868
  56.6 30.6 %copy-start.2 = (f32[2048]{0:T(1024)S(1)}, f32[2048]{0:T(1024)}, u32[]{:S(2)}) copy-start(f32[2048]{0:T(1024)} %param.22) | copy-start | bytes 24580
  58.5 126.1 %copy-start.3 = (f32[2048]{0:T(1024)S(1)}, f32[2048]{0:T(1024)}, u32[]{:S(2)}) copy-start(f32[2048]{0:T(1024)} %param.23) | copy-start | bytes 24580
  59.6 125.0 %all-gather.6.cloned.1.call-start = ((), (), s32[]{:S(2)}) async-start(), calls=%async_computation | async-start | bytes 6553600 | tf_op jit(solution)/shard_map/all_gather | solution.py:121
  60.4 222.2 %all-gather.10.cloned.1.call-start = ((), (), s32[]{:S(2)}) async-start(), calls=%async_computation.2 | async-start | bytes 6553600 | tf_op jit(solution)/shard_map/all_gather | solution.py:132
  61.1 319.3 %all-gather.8.cloned.1.call-start = ((), (), s32[]{:S(2)}) async-start(), calls=%async_computation.1 | async-start | bytes 6553600 | tf_op jit(solution)/shard_map/all_gather | solution.py:126
  61.7 357.9 %all-reduce.2.cloned.1.call-start = ((), (), s32[]{:S(2)}) async-start(), calls=%async_computation.3 | async-start | bytes 1048576 | tf_op jit(solution)/shard_map/psum | solution.py:136
  188.0 232.8 %copy-start.4 = (f32[2048]{0:T(1024)S(1)}, f32[2048]{0:T(1024)}, u32[]{:S(2)}) copy-start(f32[2048]{0:T(1024)} %param.24) | copy-start | bytes 24580
Sparse Core Ops, SparseCore 0:
  59.7 25.1 all-gather.11
  86.5 98.0 all-gather.5
  186.2 96.3 all-gather.9
  284.0 96.3 all-gather.7
  387.8 31.7 all-reduce.1
